TPU v7x, 256 devices: a whole 4x4x8 slice. The times are simulated.
256 devices in a mesh: sp: 16 (over y, x), tp: 16 (over z, core).
Axes of the slice: x: 4, y: 4, z: 8, core: 2. Of those that a mesh axis runs over, the one named last changes fastest.
Arguments:
- saved_input: bfloat16 [4096, 2048], P('sp'), may hold values from -6 to 6
- cotangent: bfloat16 [4096, 2048], P('sp'), may hold values from -6 to 6
- expert_ids: int32 [4096, 2], P('sp'), may hold values from 0 to 15, all different within a row; in each aligned block of 256 rows (0 to 255, 256 to 511, ...) at most 64 rows name the same one
- route_weight: float32 [4096, 2], P('sp'), may hold values from 0.1 to 0.9
- w_gate: bfloat16 [16, 2048, 6144], P('sp', None, 'tp'), may hold values from -0.125 to 0.125
- w_up: bfloat16 [16, 2048, 6144], P('sp', None, 'tp'), may hold values from -0.125 to 0.125
- w_down: bfloat16 [16, 6144, 2048], P('sp', 'tp'), may hold values from -0.078125 to 0.078125
- w_out: bfloat16 [2048, 2048], P(None, 'tp'), may hold values from -0.125 to 0.125
- channel_gain: float32 [2048], P('tp'), may hold values from 0.1 to 1.9
- conv_taps: float32 [31, 2048], P(None, 'tp'), may hold values from -1 to 1
- glu_value: bfloat16 [2048, 4096], P('tp', 'sp'), may hold values from -6 to 6
- glu_gate: bfloat16 [2048, 4096], P('tp', 'sp'), may hold values from -8 to 8
- conv_out: bfloat16 [2048, 4096], P('tp', 'sp'), may hold values from -6 to 6
- norm_mean: float32 [4096], P('sp'), may hold values from -3 to 3
- norm_rstd: float32 [4096], P('sp'), may hold values from 0.5 to 2
Outputs:
- gate_grad: bfloat16 [16, 2048, 6144], P('sp', None, 'tp')
- up_grad: bfloat16 [16, 2048, 6144], P('sp', None, 'tp')
- down_grad: bfloat16 [16, 6144, 2048], P('sp', 'tp')
- proj_grad: float32 [2048, 2048], P('sp', 'tp')
- value_grad: bfloat16 [2048, 4096], P('tp', 'sp')
- gate_in_grad: bfloat16 [2048, 4096], P('tp', 'sp')
Inputs may be any that keep to these rules, and one draw needn't show every extreme that they name: `expert_ids`: the two experts of a position differ. In the positions of one block of 256, no expert is named more than 64 times, a bound that some block reaches.
All inputs are finite; a program needn't handle non-finite values.
Results may differ from a plain program's by a relative error of at most 0.018.
Values may be sent and summed in bfloat16 or wider, within the bound.
No kernel may reach another device: no remote copies, remote signals or barrier semaphores. Data moves between devices by JAX's collectives and lax.ppermute only.
A program may use at most 128 MiB of HBM per device.

v0:
```python
import jax
import jax.numpy as jnp
from jax import lax
from jax.sharding import PartitionSpec as P

D = 2048
C = 2048


def in_one_piece(arrays, axis, split_dim, concat_dim, along):
    ends, at = ([], 0)
    for a in arrays[:-1]:
        at += a.shape[along]
        ends.append(at)
    both = jnp.concatenate(arrays, axis=along)
    return tuple(
        jnp.split(
            lax.all_to_all(both, axis, split_axis=split_dim, concat_axis=concat_dim, tiled=True),
            ends,
            axis=along,
        )
    )


def cut_along(value, dim, devices):
    before, after = (value.shape[:dim], value.shape[dim + 1 :])
    return jnp.moveaxis(value.reshape(*before, devices, -1, *after), dim, 0)


def sent_and_summed(value, axis, dim):
    devices = lax.axis_size(axis)
    tiles = lax.all_to_all(cut_along(value, dim, devices), axis, 0, 0, tiled=True)
    return jnp.sum(tiles.astype(jnp.float32), axis=0)


def copy_for_each(value, axis):
    copies = jnp.broadcast_to(value, (lax.axis_size(axis), *value.shape))
    return lax.all_to_all(copies, axis, split_axis=0, concat_axis=0, tiled=True)


def of_everyone(value, axis):
    everything = copy_for_each(value, axis)
    return jnp.sum(everything, axis=0)


def in_one(arrays, axis):
    ravelled, at, gathered = (jnp.concatenate([a.reshape(-1) for a in arrays]), 0, [])
    subtotal = of_everyone(ravelled, axis)
    for a in arrays:
        gathered.append(subtotal[at : at + a.size].reshape(a.shape))
        at += a.size
    return tuple(gathered)


def from_behind(value, axis, by):
    devices = lax.axis_size(axis)
    pairs = [(i, i + by) for i in range(devices) if 0 <= i + by < devices]
    return lax.ppermute(value, axis, pairs)


def contract(left, right, left_dim, right_dim):
    return lax.dot_general(
        left, right, (((left_dim,), (right_dim,)), ((), ())), preferred_element_type=jnp.float32
    )


def expert_grads(rows_in, rows_cot, gate_weight, up_weight, down_weight):
    gate_pre = jnp.dot(rows_in, gate_weight, preferred_element_type=jnp.float32)
    up_pre = jnp.dot(rows_in, up_weight, preferred_element_type=jnp.float32)
    sigma = jax.nn.sigmoid(gate_pre)
    hidden = (gate_pre * sigma * up_pre).astype(jnp.bfloat16)
    hidden_cot = contract(rows_cot, down_weight, 1, 1)
    down_part = contract(hidden, rows_cot, 0, 0).astype(jnp.bfloat16)
    gate_cot = (hidden_cot * up_pre * sigma * (1.0 + gate_pre * (1.0 - sigma))).astype(jnp.bfloat16)
    up_cot = (hidden_cot * gate_pre * sigma).astype(jnp.bfloat16)
    gate_part = contract(rows_in, gate_cot, 0, 0).astype(jnp.bfloat16)
    up_part = contract(rows_in, up_cot, 0, 0).astype(jnp.bfloat16)
    input_cot = contract(gate_cot, gate_weight, 1, 1) + contract(up_cot, up_weight, 1, 1)
    return (gate_part, up_part, down_part, input_cot)


def on_device(
    saved_input,
    cotangent,
    expert_ids,
    route_weight,
    w_gate,
    w_up,
    w_down,
    w_out,
    channel_gain,
    conv_taps,
    glu_value,
    glu_gate,
    conv_out,
    norm_mean,
    norm_rstd,
):
    tokens_here = cotangent.shape[0]
    sp_count = lax.axis_size("sp")
    local_experts = w_gate.shape[0]
    expert_count = local_experts * sp_count
    capacity = 4 * tokens_here // expert_count
    pairs = expert_ids.reshape(2 * tokens_here)
    onehot = (pairs[:, None] == jnp.arange(expert_count, dtype=jnp.int32)[None, :]).astype(
        jnp.int32
    )
    before = jnp.cumsum(onehot, axis=0) - onehot
    target = pairs * capacity + jnp.sum(before * onehot, axis=1)
    owner = (
        jnp.zeros((expert_count * capacity,), jnp.int32)
        .at[target]
        .set(jnp.arange(2 * tokens_here, dtype=jnp.int32) + 1)
    )
    filled = (owner > 0)[:, None]
    pair_index = jnp.maximum(owner - 1, 0)
    scaled = (route_weight[:, :, None] * cotangent.astype(jnp.float32)[:, None, :]).astype(
        jnp.bfloat16
    )
    scaled = scaled.reshape(2 * tokens_here, D)
    send_cot = jnp.where(filled, scaled[pair_index], jnp.zeros_like(scaled[:1])).reshape(
        expert_count, capacity, D
    )
    send_in = jnp.where(filled, saved_input[pair_index // 2], jnp.zeros_like(saved_input[:1]))
    send_in = send_in.reshape(expert_count, capacity, D)
    rows_cot, rows_in = in_one_piece((send_cot, send_in), "sp", 0, 1, 2)
    results = [expert_grads(rows_in[0], rows_cot[0], w_gate[0], w_up[0], w_down[0])]
    gate_grad = jnp.stack([result[0] for result in results])
    up_grad = jnp.stack([result[1] for result in results])
    down_grad = jnp.stack([result[2] for result in results])
    input_cot = jnp.stack([result[3] for result in results])
    blocks = input_cot.reshape(local_experts, sp_count, capacity, D)
    share = lax.psum_scatter(
        blocks.astype(jnp.bfloat16), "tp", scatter_dimension=2, tiled=True
    ).astype(jnp.float32)
    returned = lax.all_to_all(
        share.astype(jnp.bfloat16), "sp", split_axis=1, concat_axis=0, tiled=True
    ).astype(share.dtype)
    whole = lax.all_gather(returned.astype(jnp.bfloat16), "tp", axis=2, tiled=True).astype(
        returned.dtype
    )
    routed = whole.reshape(expert_count * capacity, D)[target].reshape(tokens_here, 2, D)
    summed = jnp.sum(routed, axis=1)
    mixed_cot = (cotangent.astype(jnp.float32) + summed).astype(jnp.bfloat16)
    centered = (conv_out.astype(jnp.float32) - norm_mean[None, :]) * norm_rstd[None, :]
    normed = centered * channel_gain[:, None]
    sigma = jax.nn.sigmoid(normed)
    output_act = (normed * sigma).astype(jnp.bfloat16)
    proj_grad = sent_and_summed(contract(mixed_cot, output_act, 0, 1).astype(jnp.bfloat16), "sp", 0)
    act_cot = contract(w_out, mixed_cot, 0, 1)
    norm_cot = act_cot * sigma * (1.0 + normed * (1.0 - sigma)) * channel_gain[:, None]
    first_sum, second_sum = in_one(
        (jnp.sum(norm_cot, axis=0), jnp.sum(norm_cot * centered, axis=0)), "tp"
    )
    conv_cot = norm_rstd[None, :] * (
        norm_cot - first_sum[None, :] / C - centered * second_sum[None, :] / C
    )
    reach = conv_taps.shape[0] - 1
    rim = from_behind(conv_cot[:, :reach], "sp", -1)
    padded = jnp.concatenate([conv_cot, rim], axis=1)
    glu_cot = conv_taps[0][:, None] * padded[:, :tokens_here]
    for lag in range(1, reach + 1):
        glu_cot = glu_cot + conv_taps[lag][:, None] * padded[:, lag : lag + tokens_here]
    gate_sigma = jax.nn.sigmoid(glu_gate.astype(jnp.float32))
    value_grad = (glu_cot * gate_sigma).astype(jnp.bfloat16)
    gate_in_grad = (
        glu_cot * glu_value.astype(jnp.float32) * gate_sigma * (1.0 - gate_sigma)
    ).astype(jnp.bfloat16)
    return (gate_grad, up_grad, down_grad, proj_grad, value_grad, gate_in_grad)


def solution(mesh):
    in_specs = (
        P("sp", None),
        P("sp", None),
        P("sp", None),
        P("sp", None),
        P("sp", None, "tp"),
        P("sp", None, "tp"),
        P("sp", "tp", None),
        P(None, "tp"),
        P("tp"),
        P(None, "tp"),
        P("tp", "sp"),
        P("tp", "sp"),
        P("tp", "sp"),
        P("sp"),
        P("sp"),
    )
    out_specs = (
        P("sp", None, "tp"),
        P("sp", None, "tp"),
        P("sp", "tp", None),
        P("sp", "tp"),
        P("tp", "sp"),
        P("tp", "sp"),
    )
    return jax.shard_map(
        on_device, mesh=mesh, in_specs=in_specs, out_specs=out_specs, check_vma=False
    )
```

profile of v0, /device:TPU:24, one launch (start us, length us, event | category | flops | bytes accessed | tf_op | source)
XLA Modules:
  0.0 370.5 jit_solution(13635867785435302561)
XLA Ops:
  7.2 0.0 copy-start
  7.2 0.0 reduce-scatter.2.cloned.1.call-start
  7.2 0.8 broadcast_multiply_fusion
  8.0 0.8 copy.65
  8.8 0.1 eq.25
  9.0 0.1 eq.29
  9.1 0.1 copy.64
  9.3 0.1 mul.436
  9.4 1.2 reduce-window.6
  10.6 0.2 slice_reduce_fusion
  10.9 0.1 fusion.114
  11.0 2.4 scatter_custom_fusion
  13.5 5.3 %mul.440 = f32[256,2,2048]{2,1,0:T(2,128)} broadcast(bf16[256,2048]{1,0:T(8,128)(2,1)} %param.16), dimensions={0,2} | broadcast | bytes 5242880 | tf_op jit(solution)/shard_map/mul | solution.py:117
  18.8 6.1 %mul.441 = f32[512,2048]{1,0:T(8,128)} reshape(f32[256,2,2048]{2,1,0:T(2,128)} %mul.440) | data formatting | bytes 8388608 | tf_op jit(solution)/shard_map/mul | solution.py:117
  24.9 0.1 copy.68
  25.0 0.1 mul.438
  25.2 0.1 broadcast_in_dim.46
  25.2 3.8 %multiply_convert_fusion = bf16[512,2048]{1,0:T(8,128)(2,1)} fusion(f32[512,2048]{1,0:T(8,128)} %mul.441, f32[512]{0:T(512)S(1)} %mul.438), kind=kLoop, calls=%fused_computation.8 | loop fusion | flops 2097152 | bytes 6293504 | tf_op jit(solution)/shard_map/convert_element_type | solution.py:117
  29.0 10.8 %gather_fusion = bf16[1024,2048]{1,0:T(8,128)(2,1)} fusion(bf16[512,2048]{1,0:T(8,128)(2,1)} %multiply_convert_fusion, s32[1024]{0:T(1024)S(1)} %get-tuple-element.73), kind=kCustom, calls=%fused_computation | custom fusion | bytes 8392704 | tf_op jit(solution)/shard_map/gather | solution.py:121
  39.8 6.0 %gather_fusion.1 = bf16[1024,2048]{1,0:T(8,128)(2,1)} fusion(bf16[256,2048]{1,0:T(8,128)(2,1)S(1)} %copy-done.2, s32[1024]{0:T(1024)S(1)} %get-tuple-element.74), kind=kCustom, calls=%fused_computation.1 | custom fusion | bytes 8392704 | tf_op jit(solution)/shard_map/gather | solution.py:124
  45.8 5.8 %broadcast_select_fusion.1 = (bf16[16,64,2048]{2,1,0:T(8,128)(2,1)}, bf16[16,64,2048]{2,1,0:T(8,128)(2,1)}) fusion(bf16[16,64,2048]{2,1,0:T(8,128)(2,1)} %bitcast.144, pred[16,64]{1,0:T(8,128)(4,1)S(1)} %broadcast_in_dim.46, bf16[16,64,2048]{2,1,0:T(8,128)(2,1)} %bitcast.145), kind=kLoop, calls=%fused_computation.10 | loop fusion | flops 4194304 | bytes 16778240 | tf_op jit(solution)/shard_map/jit(_where)/select_n | solution.py:121
  51.6 7.8 %pad_maximum_fusion = bf16[16,64,4096]{2,1,0:T(8,128)(2,1)} fusion(bf16[16,64,2048]{2,1,0:T(8,128)(2,1)} %get-tuple-element.78, bf16[16,64,2048]{2,1,0:T(8,128)(2,1)} %get-tuple-element.77), kind=kLoop, calls=%fused_computation.4 | loop fusion | flops 16777216 | bytes 16777216 | tf_op jit(solution)/shard_map/concatenate | solution.py:15
  59.4 101.1 %all_to_all.35 = bf16[16,64,4096]{2,1,0:T(8,128)(2,1)S(1)} all-to-all(bf16[16,64,4096]{2,1,0:T(8,128)(2,1)} %pad_maximum_fusion), channel_id=1, replica_groups=mesh['sp'=16,'tp'=16] {'sp'}, dimensions={0} | all-to-all | bytes 16777216 | tf_op jit(solution)/shard_map/all_to_all | solution.py:18
  160.6 2.3 fusion.3
  162.9 0.2 copy-done.5
  163.1 2.3 fusion.4
  165.5 0.2 copy-done.15
  165.7 2.8 multiply_convert_fusion.2
  168.5 2.4 fusion.8
  170.9 2.4 add_convert_fusion
  173.3 4.3 %copy.69 = bf16[1,16,64,2048]{3,1,0,2:T(8,128)(2,1)} copy(bf16[1,16,64,2048]{3,2,1,0:T(8,128)(2,1)S(1)} %bitcast.146) | data formatting | bytes 8388608 | tf_op jit(solution)/shard_map/convert_element_type | solution.py:134
  177.6 0.0 reduce-scatter.2.cloned.1.call-update
  177.6 0.0 all-gather.3.cloned.1.call-start
  177.6 64.5 %reduce-scatter.2.cloned.1.call-done = bf16[1,16,4,2048]{3,1,0,2:T(8,128)(2,1)} async-done(((bf16[1,16,64,2048]{3,1,0,2:T(8,128)(2,1)}), bf16[1,16,4,2048]{3,1,0,2:T(8,128)(2,1)}) %reduce-scatter.2.cloned.1.call-update) | async-done | bytes 262160 | tf_op jit(solution)/shard_map/reduce_scatter | solution.py:133
  242.2 1.2 copy.70
  243.3 13.6 %all_to_all.36 = bf16[1,16,4,2048]{3,2,0,1:T(4,128)(2,1)S(1)} all-to-all(bf16[1,16,4,2048]{3,2,0,1:T(4,128)(2,1)S(1)} %copy.70), channel_id=1, replica_groups=mesh['sp'=16,'tp'=16] {'sp'}, dimensions={1} | all-to-all | bytes 524288 | tf_op jit(solution)/shard_map/all_to_all | solution.py:136
  256.9 0.9 copy.71
  257.8 0.0 all-gather.3.cloned.1.call-update
  257.8 0.1 copy.73
  257.9 0.1 copy.76
  258.1 0.1 copy.75
  258.3 0.0 copy-start.19
  258.3 5.9 %fusion.5 = bf16[1,2048,384]{2,1,0:T(8,128)(2,1)} fusion(bf16[1024,384]{1,0:T(8,128)(2,1)S(1)} %get-tuple-element.41, bf16[1,1024,4096]{2,1,0:T(8,128)(2,1)} %bitcast.150), kind=kOutput, calls=%fused_computation.18 | convolution fusion | flops 1611399168 | bytes 6553600 | tf_op jit(solution)/shard_map/dot_general | solution.py:62
  264.1 5.4 %fusion.7 = bf16[1,384,2048]{2,1,0:T(8,128)(2,1)} fusion(bf16[1,1024,4096]{2,1,0:T(8,128)(2,1)} %bitcast.151, f32[1024,384]{1,0:T(8,128)S(1)} %copy-done.19, f32[1024,384]{1,0:T(8,128)S(1)} %copy-done.17), kind=kOutput, calls=%fused_computation.20 | convolution fusion | flops 1613758464 | bytes 8912896 | tf_op jit(solution)/shard_map/dot_general | solution.py:62
  269.5 26.8 %all-gather.3.cloned.1.call-done = bf16[1,16,64,2048]{3,1,0,2:T(8,128)(2,1)} async-done(((bf16[1,16,4,2048]{3,1,0,2:T(8,128)(2,1)}), bf16[1,16,64,2048]{3,1,0,2:T(8,128)(2,1)}) %all-gather.3.cloned.1.call-update) | async-done | bytes 4194320 | tf_op jit(solution)/shard_map/all_gather | solution.py:139
  296.3 7.8 %copy.72 = f32[1,16,64,2048]{3,2,1,0:T(8,128)} copy(bf16[1,16,64,2048]{3,1,0,2:T(8,128)(2,1)} %all-gather.3.cloned.1.call-done) | data formatting | bytes 12582912 | tf_op jit(solution)/shard_map/reshape | solution.py:142
  304.2 8.8 %gather_fusion.2 = f32[512,2048]{1,0:T(8,128)} fusion(f32[1024,2048]{1,0:T(8,128)} %bitcast.143, s32[1024]{0:T(1024)S(1)} %pad_clamp_fusion), kind=kCustom, calls=%fused_computation.2 | custom fusion | bytes 8390656 | tf_op jit(solution)/shard_map/gather | solution.py:142
  312.9 6.0 %reshape.159 = f32[256,2,2048]{2,1,0:T(2,128)} reshape(f32[512,2048]{1,0:T(8,128)} %gather_fusion.2) | data formatting | bytes 8388608 | tf_op jit(solution)/shard_map/reshape | solution.py:142
  319.0 0.0 copy-start.3
  319.0 0.0 copy-start.6
  319.0 8.6 %reduce_sum.58 = f32[256,2048]{1,0:T(8,128)} reduce(f32[256,2,2048]{2,1,0:T(2,128)} %reshape.159, f32[]{:T(128)} %constant.44.clone.1), dimensions={1}, to_apply=%region_5.6 | reduce | flops 524288 | bytes 6291460 | tf_op jit(solution)/shard_map/reduce_sum | solution.py:143
  327.7 2.1 fusion.123
  329.8 0.6 broadcast_in_dim.51
  330.5 4.4 %all-to-all-start.3 = ((f32[16,1,512]{2,1,0:T(1,128)}), f32[16,1,512]{2,1,0:T(1,128)S(1)}, u32[]{:S(2)}, u32[]{:S(2)}) async-start(f32[16,1,512]{2,1,0:T(1,128)} %broadcast_in_dim.51), calls=%async_computation.4 | async-start | bytes 65536 | tf_op jit(solution)/shard_map/all_to_all | solution.py:38
  334.9 3.1 convolution_convert_fusion.2
  337.9 4.6 %all-to-all-done.3 = f32[16,1,512]{2,1,0:T(1,128)S(1)} async-done(((f32[16,1,512]{2,1,0:T(1,128)}), f32[16,1,512]{2,1,0:T(1,128)S(1)}, u32[]{:S(2)}, u32[]{:S(2)}) %all-to-all-start.3) | async-done | bytes 32800 | tf_op jit(solution)/shard_map/all_to_all | solution.py:38
  342.5 7.2 %all-to-all-start.2 = ((bf16[16,128,128]{2,1,0:T(8,128)(2,1)}), bf16[16,128,128]{2,1,0:T(8,128)(2,1)S(1)}, u32[]{:S(2)}, u32[]{:S(2)}) async-start(bf16[16,128,128]{2,1,0:T(8,128)(2,1)} %bitcast.16), calls=%async_computation.3 | async-start | bytes 1048576 | tf_op jit(solution)/shard_map/all_to_all | solution.py:32
  349.8 0.2 subtract_multiply_fusion
  350.0 4.9 %collective-permute-start = (f32[128,30]{0,1:T(8,128)S(1)}, f32[128,30]{0,1:T(8,128)S(1)}, u32[]{:S(2)}, u32[]{:S(2)}) collective-permute-start(f32[128,30]{0,1:T(8,128)S(1)} %slice.271), channel_id=1, source_target_pairs={{16,0},{32,16},{48,32},{64,48},{80,64},{96,80},{112,96},{128,112},... | collective-permute-start | bytes 46088 | tf_op jit(solution)/shard_map/ppermute | solution.py:58
  354.9 5.8 %fusion.6 = bf16[1,2048,384]{2,1,0:T(8,128)(2,1)} fusion(bf16[1024,384]{1,0:T(8,128)(2,1)S(1)} %get-tuple-element.40, bf16[1,1024,4096]{2,1,0:T(8,128)(2,1)} %bitcast.152), kind=kOutput, calls=%fused_computation.19 | convolution fusion | flops 1611399168 | bytes 6553600 | tf_op jit(solution)/shard_map/dot_general | solution.py:62
  360.8 0.4 multiply_convert_fusion.5
  361.2 0.7 copy.77
  362.0 0.7 copy.78
  362.7 0.7 convert_reduce_fusion
  (51 shorter events, 0.3 us)
Async XLA Ops:
  7.2 153.4 %copy-start = (bf16[1,2048,384]{2,1,0:T(8,128)(2,1)S(1)}, bf16[1,2048,384]{2,1,0:T(8,128)(2,1)}, u32[]{:S(2)}) copy-start(bf16[1,2048,384]{2,1,0:T(8,128)(2,1)} %param.19) | copy-start | bytes 4718596
  7.2 235.0 %reduce-scatter.2.cloned.1.call-start = ((), (), s32[]{:S(2)}) async-start(), calls=%async_computation.5 | async-start | bytes 4456448 | tf_op jit(solution)/shard_map/reduce_scatter | solution.py:133
  18.8 6.1 %copy-start.13 = (f32[256,2]{0,1:T(2,128)S(1)}, f32[256,2]{0,1:T(2,128)}, u32[]{:S(2)}) copy-start(f32[256,2]{0,1:T(2,128)} %param.18) | copy-start | bytes 6148
  29.0 10.8 %copy-start.2 = (bf16[256,2048]{1,0:T(8,128)(2,1)S(1)}, bf16[256,2048]{1,0:T(8,128)(2,1)}, u32[]{:S(2)}) copy-start(bf16[256,2048]{1,0:T(8,128)(2,1)} %param.15) | copy-start | bytes 3145732
  160.6 4.9 %copy-start.4 = (bf16[16,64,4096]{2,1,0:T(8,128)(2,1)}, bf16[16,64,4096]{2,1,0:T(8,128)(2,1)S(1)}, u32[]{:S(2)}) copy-start(bf16[16,64,4096]{2,1,0:T(8,128)(2,1)S(1)} %all_to_all.35) | copy-start | bytes 25165828
  160.6 2.6 copy-start.5
  163.1 2.4 copy-start.16
  163.1 2.6 copy-start.15
  165.7 2.8 copy-start.18
  177.6 80.2 %copy-start.7 = (bf16[128,256]{1,0:T(8,128)(2,1)S(1)}, bf16[128,256]{1,0:T(8,128)(2,1)}, u32[]{:S(2)}) copy-start(bf16[128,256]{1,0:T(8,128)(2,1)} %param.27) | copy-start | bytes 196612
  177.6 80.4 %copy-start.8 = (bf16[128,256]{1,0:T(8,128)(2,1)S(1)}, bf16[128,256]{1,0:T(8,128)(2,1)}, u32[]{:S(2)}) copy-start(bf16[128,256]{1,0:T(8,128)(2,1)} %param.25) | copy-start | bytes 196612
  177.6 80.5 %copy-start.9 = (bf16[128,256]{1,0:T(8,128)(2,1)S(1)}, bf16[128,256]{1,0:T(8,128)(2,1)}, u32[]{:S(2)}) copy-start(bf16[128,256]{1,0:T(8,128)(2,1)} %param.26) | copy-start | bytes 196612
  177.6 80.6 %copy-start.10 = (f32[31,128]{1,0:T(8,128)S(1)}, f32[31,128]{1,0:T(8,128)}, u32[]{:S(2)}) copy-start(f32[31,128]{1,0:T(8,128)} %param.24) | copy-start | bytes 47620
  177.6 118.7 %all-gather.3.cloned.1.call-start = ((), (), s32[]{:S(2)}) async-start(), calls=%async_computation.6 | async-start | bytes 4456448 | tf_op jit(solution)/shard_map/all_gather | solution.py:139
  258.2 5.9 %copy-start.17 = (f32[1024,384]{1,0:T(8,128)S(1)}, f32[1024,384]{1,0:T(8,128)}, u32[]{:S(2)}) copy-start(f32[1024,384]{1,0:T(8,128)} %copy-done.16) | copy-start | bytes 4718596
  258.3 5.9 %copy-start.19 = (f32[1024,384]{1,0:T(8,128)S(1)}, f32[1024,384]{1,0:T(8,128)}, u32[]{:S(2)}) copy-start(f32[1024,384]{1,0:T(8,128)} %copy-done.18) | copy-start | bytes 4718596
  319.0 8.7 %copy-start.3 = (bf16[256,2048]{1,0:T(8,128)(2,1)S(1)}, bf16[256,2048]{1,0:T(8,128)(2,1)}, u32[]{:S(2)}) copy-start(bf16[256,2048]{1,0:T(8,128)(2,1)} %param.16) | copy-start | bytes 3145732
  319.0 8.7 %copy-start.6 = (bf16[2048,128]{1,0:T(8,128)(2,1)S(1)}, bf16[2048,128]{1,0:T(8,128)(2,1)}, u32[]{:S(2)}) copy-start(bf16[2048,128]{1,0:T(8,128)(2,1)} %param.22) | copy-start | bytes 1572868
  319.0 8.7 %copy-start.11 = (f32[256]{0:T(256)S(1)}, f32[256]{0:T(256)}, u32[]{:S(2)}) copy-start(f32[256]{0:T(256)} %param.29) | copy-start | bytes 3076
  319.0 8.7 %copy-start.12 = (f32[256]{0:T(256)S(1)}, f32[256]{0:T(256)}, u32[]{:S(2)}) copy-start(f32[256]{0:T(256)} %param.28) | copy-start | bytes 3076
  319.0 8.7 %copy-start.14 = (f32[128]{0:T(128)S(1)}, f32[128]{0:T(128)}, u32[]{:S(2)}) copy-start(f32[128]{0:T(128)} %param.23) | copy-start | bytes 1540
  330.5 12.1 %all-to-all-start.3 = ((f32[16,1,512]{2,1,0:T(1,128)}), f32[16,1,512]{2,1,0:T(1,128)S(1)}, u32[]{:S(2)}, u32[]{:S(2)}) async-start(f32[16,1,512]{2,1,0:T(1,128)} %broadcast_in_dim.51), calls=%async_computation.4 | async-start | bytes 65536 | tf_op jit(solution)/shard_map/all_to_all | solution.py:38
  342.5 20.2 %all-to-all-start.2 = ((bf16[16,128,128]{2,1,0:T(8,128)(2,1)}), bf16[16,128,128]{2,1,0:T(8,128)(2,1)S(1)}, u32[]{:S(2)}, u32[]{:S(2)}) async-start(bf16[16,128,128]{2,1,0:T(8,128)(2,1)} %bitcast.16), calls=%async_computation.3 | async-start | bytes 1048576 | tf_op jit(solution)/shard_map/all_to_all | solution.py:32
  350.0 10.7 %collective-permute-start = (f32[128,30]{0,1:T(8,128)S(1)}, f32[128,30]{0,1:T(8,128)S(1)}, u32[]{:S(2)}, u32[]{:S(2)}) collective-permute-start(f32[128,30]{0,1:T(8,128)S(1)} %slice.271), channel_id=1, source_target_pairs={{16,0},{32,16},{48,32},{64,48},{80,64},{96,80},{112,96},{128,112},... | collective-permute-start | bytes 46088 | tf_op jit(solution)/shard_map/ppermute | solution.py:58
  354.9 8.5 %copy-start.1 = (bf16[1,2048,384]{2,1,0:T(8,128)(2,1)S(1)}, bf16[1,2048,384]{2,1,0:T(8,128)(2,1)}, u32[]{:S(2)}) copy-start(bf16[1,2048,384]{2,1,0:T(8,128)(2,1)} %param.19) | copy-start | bytes 4718596
Sparse Core Ops, SparseCore 0:
  177.7 64.3 reduce-scatter.1
  257.9 38.3 all-gather.2
where the time goes:
time: 377 us; the launch traced here: 370 us
  blocking collectives  115 us (31%)
  waiting for transfers between devices  95.9 us (25%)
  local copies, waits for them, and re-layouts  64.5 us (17%)
  matrix products  34.5 us (9%)
  other arithmetic  29.5 us (8%)
  starting transfers between devices  16.6 us (4%)
  between operations  14.6 us (4%)
    all_to_all x1, blocking collectives, in_one_piece(): lax.all_to_all(both, axis, split_axis=split_dim, concat_axis=concat_dim,...  101 us
    reduce_scatter x1, waiting for transfers between devices, on_device(): lax.psum_scatter(blocks.astype(jnp.bfloat16), 'tp', scatter_dimension=2,...  64.5 us
    dot_general x8, matrix products, contract(): lax.dot_general(left, right, (((left_dim,), (right_dim,)), ((), ())), pre...  29.9 us
    all_gather x1, waiting for transfers between devices, on_device(): lax.all_gather(returned.astype(jnp.bfloat16), 'tp', axis=2, tiled=True)  26.8 us
    reshape x2, local copies, waits for them, and re-layouts, on_device(): whole.reshape(expert_count * capacity, D)[target].reshape(tokens_here, 2, D)  13.9 us
    all_to_all x1, blocking collectives, on_device(): lax.all_to_all(share.astype(jnp.bfloat16), 'sp', split_axis=1, concat_axi...  13.6 us
    mul x3, local copies, waits for them, and re-layouts, on_device(): route_weight[:, :, None] * cotangent.astype(jnp.float32)[:, None, :]  11.6 us
    gather x1, local copies, waits for them, and re-layouts, on_device(): scaled[pair_index]  10.8 us
  transfers between devices with their start and end apart: 5, of which 3 were waited for; matrix products, arithmetic and copies ran while one was open for 6% of the time, Pallas kernels for 0%

commit v1 on v0

--- a/solution.py
+++ b/solution.py
@@ -5,6 +5,13 @@
 
 D = 2048
 C = 2048
+
+
+def exchange_gather(shard, name, dim):
+    peers = lax.axis_size(name)
+    blocks = jnp.stack([shard for _ in range(peers)])
+    blocks = lax.all_to_all(blocks, name, split_axis=0, concat_axis=0)
+    return jnp.concatenate(blocks, axis=dim)
 
 
 def in_one_piece(arrays, axis, split_dim, concat_dim, along):
@@ -136,9 +143,7 @@
     returned = lax.all_to_all(
         share.astype(jnp.bfloat16), "sp", split_axis=1, concat_axis=0, tiled=True
     ).astype(share.dtype)
-    whole = lax.all_gather(returned.astype(jnp.bfloat16), "tp", axis=2, tiled=True).astype(
-        returned.dtype
-    )
+    whole = exchange_gather(returned.astype(jnp.bfloat16), "tp", 2).astype(returned.dtype)
     routed = whole.reshape(expert_count * capacity, D)[target].reshape(tokens_here, 2, D)
     summed = jnp.sum(routed, axis=1)
     mixed_cot = (cotangent.astype(jnp.float32) + summed).astype(jnp.bfloat16)

time: 377 us -> 459 us (1.22)
  waiting for transfers between devices: 95.9 us -> 152 us
  local copies, waits for them, and re-layouts: 64.5 us -> 80.3 us
  other arithmetic: 29.5 us -> 36.6 us
    all_to_all x0 -> x1, waiting for transfers between devices: none -> 82.7 us  [exchange_gather(): blocks = lax.all_to_all(blocks, name, split_axis=0, concat_axis=0)]
    all_gather x1 -> x0, waiting for transfers between devices: 26.8 us -> none  [on_device(): lax.all_gather(returned.astype(jnp.bfloat16), 'tp', axis=2, tiled=True)]
    convert_element_type x0 -> x2, local copies, waits for them, and re-layouts: none -> 20.3 us  [on_device(): exchange_gather(returned.astype(jnp.bfloat16), 'tp', 2)]
    reshape x2 -> x1, local copies, waits for them, and re-layouts: 13.9 us -> 6.03 us  [on_device(): whole.reshape(expert_count * capacity, D)[target].reshape(tokens_here, 2, D)]
    convert_element_type x0 -> x1, other arithmetic: none -> 7.07 us  [on_device(): exchange_gather(returned.astype(jnp.bfloat16), 'tp', 2)]
    all_to_all x0 -> x1, starting transfers between devices: none -> 4.69 us  [exchange_gather(): blocks = lax.all_to_all(blocks, name, split_axis=0, concat_axis=0)]
  transfers between devices with their start and end apart: 5 -> 5, of which waited for: 3 -> 3; matrix products, arithmetic and copies ran while one was open for 6% -> 5% of each run, Pallas kernels for 0% -> 0%
where the time goes in v1:
time: 459 us; the launch traced here: 453 us
  waiting for transfers between devices  152 us (33%)
  blocking collectives  115 us (25%)
  local copies, waits for them, and re-layouts  80.3 us (17%)
  other arithmetic  36.6 us (8%)
  matrix products  34.4 us (7%)
  starting transfers between devices  20 us (4%)
  between operations  14.6 us (3%)
    all_to_all x1, blocking collectives, in_one_piece(): lax.all_to_all(both, axis, split_axis=split_dim, concat_axis=concat_dim,...  101 us
    all_to_all x1, waiting for transfers between devices, exchange_gather(): blocks = lax.all_to_all(blocks, name, split_axis=0, concat_axis=0)  82.7 us
    reduce_scatter x1, waiting for transfers between devices, on_device(): lax.psum_scatter(blocks.astype(jnp.bfloat16), 'tp', scatter_dimension=2,...  64.6 us
    dot_general x8, matrix products, contract(): lax.dot_general(left, right, (((left_dim,), (right_dim,)), ((), ())), pre...  29.7 us
    convert_element_type x2, local copies, waits for them, and re-layouts, on_device(): exchange_gather(returned.astype(jnp.bfloat16), 'tp', 2)  20.3 us
    all_to_all x1, blocking collectives, on_device(): lax.all_to_all(share.astype(jnp.bfloat16), 'sp', split_axis=1, concat_axi...  13.6 us
    mul x3, local copies, waits for them, and re-layouts, on_device(): route_weight[:, :, None] * cotangent.astype(jnp.float32)[:, None, :]  11.6 us
    gather x1, local copies, waits for them, and re-layouts, on_device(): scaled[pair_index]  10.8 us
  transfers between devices with their start and end apart: 5, of which 3 were waited for; matrix products, arithmetic and copies ran while one was open for 5% of the time, Pallas kernels for 0%

profile of v1, /device:TPU:24, one launch (start us, length us, event | category | flops | bytes accessed | tf_op | source)
XLA Modules:
  0.0 452.5 jit_solution(16937218943977168284)
XLA Ops:
  7.2 0.0 copy-start
  7.2 0.0 reduce-scatter.2.cloned.1.call-start
  7.2 0.8 broadcast_multiply_fusion
  8.0 0.8 copy.63
  8.8 0.1 eq.25
  9.0 0.1 eq.29
  9.1 0.1 copy.62
  9.3 0.1 mul.436
  9.4 1.2 reduce-window.6
  10.6 0.2 slice_reduce_fusion
  10.9 0.1 fusion.114
  11.0 2.4 scatter_custom_fusion
  13.5 5.3 %mul.440 = f32[256,2,2048]{2,1,0:T(2,128)} broadcast(bf16[256,2048]{1,0:T(8,128)(2,1)} %param.16), dimensions={0,2} | broadcast | bytes 5242880 | tf_op jit(solution)/shard_map/mul | solution.py:124
  18.8 6.1 %mul.441 = f32[512,2048]{1,0:T(8,128)} reshape(f32[256,2,2048]{2,1,0:T(2,128)} %mul.440) | data formatting | bytes 8388608 | tf_op jit(solution)/shard_map/mul | solution.py:124
  24.9 0.1 copy.66
  25.0 0.1 mul.438
  25.2 0.1 broadcast_in_dim.46
  25.2 3.8 multiply_convert_fusion
  29.0 10.8 %gather_fusion = bf16[1024,2048]{1,0:T(8,128)(2,1)} fusion(bf16[512,2048]{1,0:T(8,128)(2,1)} %multiply_convert_fusion, s32[1024]{0:T(1024)S(1)} %get-tuple-element.73), kind=kCustom, calls=%fused_computation | custom fusion | bytes 8392704 | tf_op jit(solution)/shard_map/gather | solution.py:128
  39.8 6.0 %gather_fusion.1 = bf16[1024,2048]{1,0:T(8,128)(2,1)} fusion(bf16[256,2048]{1,0:T(8,128)(2,1)S(1)} %copy-done.2, s32[1024]{0:T(1024)S(1)} %get-tuple-element.74), kind=kCustom, calls=%fused_computation.1 | custom fusion | bytes 8392704 | tf_op jit(solution)/shard_map/gather | solution.py:131
  45.8 5.8 %broadcast_select_fusion.1 = (bf16[16,64,2048]{2,1,0:T(8,128)(2,1)}, bf16[16,64,2048]{2,1,0:T(8,128)(2,1)}) fusion(bf16[16,64,2048]{2,1,0:T(8,128)(2,1)} %bitcast.147, pred[16,64]{1,0:T(8,128)(4,1)S(1)} %broadcast_in_dim.46, bf16[16,64,2048]{2,1,0:T(8,128)(2,1)} %bitcast.148), kind=kLoop, calls=%fused_computation.11 | loop fusion | flops 4194304 | bytes 16778240 | tf_op jit(solution)/shard_map/jit(_where)/select_n | solution.py:128
  51.6 7.8 %pad_maximum_fusion = bf16[16,64,4096]{2,1,0:T(8,128)(2,1)} fusion(bf16[16,64,2048]{2,1,0:T(8,128)(2,1)} %get-tuple-element.78, bf16[16,64,2048]{2,1,0:T(8,128)(2,1)} %get-tuple-element.77), kind=kLoop, calls=%fused_computation.4 | loop fusion | flops 16777216 | bytes 16777216 | tf_op jit(solution)/shard_map/concatenate | solution.py:22
  59.4 101.1 %all_to_all.37 = bf16[16,64,4096]{2,1,0:T(8,128)(2,1)S(1)} all-to-all(bf16[16,64,4096]{2,1,0:T(8,128)(2,1)} %pad_maximum_fusion), channel_id=1, replica_groups=mesh['sp'=16,'tp'=16] {'sp'}, dimensions={0} | all-to-all | bytes 16777216 | tf_op jit(solution)/shard_map/all_to_all | solution.py:25
  160.6 2.3 fusion.3
  162.9 0.2 copy-done.5
  163.1 2.3 fusion.4
  165.5 0.2 copy-done.15
  165.7 2.8 multiply_convert_fusion.2
  168.5 2.4 fusion.8
  170.9 2.4 add_convert_fusion
  173.3 4.3 copy.67
  177.5 0.0 reduce-scatter.2.cloned.1.call-update
  177.6 64.6 %reduce-scatter.2.cloned.1.call-done = bf16[1,16,4,2048]{3,1,0,2:T(8,128)(2,1)} async-done(((bf16[1,16,64,2048]{3,1,0,2:T(8,128)(2,1)}), bf16[1,16,4,2048]{3,1,0,2:T(8,128)(2,1)}) %reduce-scatter.2.cloned.1.call-update) | async-done | bytes 262160 | tf_op jit(solution)/shard_map/reduce_scatter | solution.py:140
  242.1 1.2 copy.68
  243.3 13.6 %all_to_all.38 = bf16[1,16,4,2048]{3,2,0,1:T(4,128)(2,1)S(1)} all-to-all(bf16[1,16,4,2048]{3,2,0,1:T(4,128)(2,1)S(1)} %copy.68), channel_id=1, replica_groups=mesh['sp'=16,'tp'=16] {'sp'}, dimensions={1} | all-to-all | bytes 524288 | tf_op jit(solution)/shard_map/all_to_all | solution.py:143
  256.9 4.1 stack.14
  261.0 4.7 %all-to-all-start.2 = ((bf16[16,16,1,4,2048]{4,3,1,2,0:T(4,128)(2,1)}), bf16[16,16,1,4,2048]{4,3,1,2,0:T(4,128)(2,1)}, u32[]{:S(2)}, u32[]{:S(2)}) async-start(bf16[16,16,1,4,2048]{4,3,1,2,0:T(4,128)(2,1)} %stack.14), calls=%async_computation.3 | async-start | bytes 8388608 | tf_op jit(solution)/shard_map/all_to_all | solution.py:13
  265.7 0.1 copy.70
  265.8 0.1 copy.73
  266.0 0.1 copy.72
  266.1 0.0 copy-start.17
  266.1 0.0 copy-start.19
  266.2 5.9 %fusion.5 = bf16[1,2048,384]{2,1,0:T(8,128)(2,1)} fusion(bf16[1024,384]{1,0:T(8,128)(2,1)S(1)} %get-tuple-element.41, bf16[1,1024,4096]{2,1,0:T(8,128)(2,1)} %bitcast.153), kind=kOutput, calls=%fused_computation.19 | convolution fusion | flops 1611399168 | bytes 6553600 | tf_op jit(solution)/shard_map/dot_general | solution.py:69
  272.0 5.2 %fusion.7 = bf16[1,384,2048]{2,1,0:T(8,128)(2,1)} fusion(bf16[1,1024,4096]{2,1,0:T(8,128)(2,1)} %bitcast.154, f32[1024,384]{1,0:T(8,128)S(1)} %copy-done.19, f32[1024,384]{1,0:T(8,128)S(1)} %copy-done.17), kind=kOutput, calls=%fused_computation.21 | convolution fusion | flops 1613758464 | bytes 8912896 | tf_op jit(solution)/shard_map/dot_general | solution.py:69
  277.3 82.7 %all-to-all-done.2 = bf16[16,16,1,4,2048]{4,3,1,2,0:T(4,128)(2,1)} async-done(((bf16[16,16,1,4,2048]{4,3,1,2,0:T(4,128)(2,1)}), bf16[16,16,1,4,2048]{4,3,1,2,0:T(4,128)(2,1)}, u32[]{:S(2)}, u32[]{:S(2)}) %all-to-all-start.2) | async-done | bytes 4194336 | tf_op jit(solution)/shard_map/all_to_all | solution.py:13
  359.9 7.1 %convert_bitcast_fusion = f32[16,1,16,4,2048]{4,3,0,1,2:T(4,128)} fusion(bf16[16,16,1,4,2048]{4,3,1,2,0:T(4,128)(2,1)} %all-to-all-done.2), kind=kLoop, calls=%fused_computation.5 | loop fusion | flops 2097152 | bytes 12582912 | tf_op jit(solution)/shard_map/convert_element_type | solution.py:146
  367.0 10.3 %copy.69 = f32[16,1,16,4,2048]{4,3,2,0,1:T(4,128)} copy(f32[16,1,16,4,2048]{4,3,0,1,2:T(4,128)} %convert_bitcast_fusion) | data formatting | bytes 16777216 | tf_op jit(solution)/shard_map/convert_element_type | solution.py:146
  377.3 10.0 %reshape.166 = f32[1024,2048]{1,0:T(8,128)} reshape(f32[16,1,16,4,2048]{4,3,2,0,1:T(4,128)} %copy.69) | data formatting | bytes 16777216 | tf_op jit(solution)/shard_map/convert_element_type | solution.py:146
  387.3 8.8 %gather_fusion.2 = f32[512,2048]{1,0:T(8,128)} fusion(f32[1024,2048]{1,0:T(8,128)} %reshape.166, s32[1024]{0:T(1024)S(1)} %pad_clamp_fusion), kind=kCustom, calls=%fused_computation.2 | custom fusion | bytes 8390656 | tf_op jit(solution)/shard_map/gather | solution.py:147
  396.1 6.0 %reshape.164 = f32[256,2,2048]{2,1,0:T(2,128)} reshape(f32[512,2048]{1,0:T(8,128)} %gather_fusion.2) | data formatting | bytes 8388608 | tf_op jit(solution)/shard_map/reshape | solution.py:147
  402.2 8.6 %reduce_sum.58 = f32[256,2048]{1,0:T(8,128)} reduce(f32[256,2,2048]{2,1,0:T(2,128)} %reshape.164, f32[]{:T(128)} %constant.44.clone.1), dimensions={1}, to_apply=%region_5.6 | reduce | flops 524288 | bytes 6291460 | tf_op jit(solution)/shard_map/reduce_sum | solution.py:148
  410.9 2.1 fusion.123
  413.0 0.6 broadcast_in_dim.51
  413.7 4.6 %all-to-all-start.4 = ((f32[16,1,512]{2,1,0:T(1,128)}), f32[16,1,512]{2,1,0:T(1,128)S(1)}, u32[]{:S(2)}, u32[]{:S(2)}) async-start(f32[16,1,512]{2,1,0:T(1,128)} %broadcast_in_dim.51), calls=%async_computation.5 | async-start | bytes 65536 | tf_op jit(solution)/shard_map/all_to_all | solution.py:45
  418.3 3.1 convolution_convert_fusion.2
  421.4 4.6 %all-to-all-done.4 = f32[16,1,512]{2,1,0:T(1,128)S(1)} async-done(((f32[16,1,512]{2,1,0:T(1,128)}), f32[16,1,512]{2,1,0:T(1,128)S(1)}, u32[]{:S(2)}, u32[]{:S(2)}) %all-to-all-start.4) | async-done | bytes 32800 | tf_op jit(solution)/shard_map/all_to_all | solution.py:45
  426.0 5.8 %all-to-all-start.3 = ((bf16[16,128,128]{2,1,0:T(8,128)(2,1)}), bf16[16,128,128]{2,1,0:T(8,128)(2,1)S(1)}, u32[]{:S(2)}, u32[]{:S(2)}) async-start(bf16[16,128,128]{2,1,0:T(8,128)(2,1)} %bitcast.17), calls=%async_computation.4 | async-start | bytes 1048576 | tf_op jit(solution)/shard_map/all_to_all | solution.py:39
  431.9 0.2 subtract_multiply_fusion
  432.1 4.9 %collective-permute-start = (f32[128,30]{0,1:T(8,128)S(1)}, f32[128,30]{0,1:T(8,128)S(1)}, u32[]{:S(2)}, u32[]{:S(2)}) collective-permute-start(f32[128,30]{0,1:T(8,128)S(1)} %slice.271), channel_id=1, source_target_pairs={{16,0},{32,16},{48,32},{64,48},{80,64},{96,80},{112,96},{128,112},... | collective-permute-start | bytes 46088 | tf_op jit(solution)/shard_map/ppermute | solution.py:65
  437.0 5.8 %fusion.6 = bf16[1,2048,384]{2,1,0:T(8,128)(2,1)} fusion(bf16[1024,384]{1,0:T(8,128)(2,1)S(1)} %get-tuple-element.40, bf16[1,1024,4096]{2,1,0:T(8,128)(2,1)} %bitcast.155), kind=kOutput, calls=%fused_computation.20 | convolution fusion | flops 1611399168 | bytes 6553600 | tf_op jit(solution)/shard_map/dot_general | solution.py:69
  442.8 0.4 multiply_convert_fusion.5
  443.3 0.7 copy.74
  444.0 0.7 copy.75
  444.8 0.7 convert_reduce_fusion
  (52 shorter events, 0.3 us)
Async XLA Ops:
  7.2 153.4 %copy-start = (bf16[1,2048,384]{2,1,0:T(8,128)(2,1)S(1)}, bf16[1,2048,384]{2,1,0:T(8,128)(2,1)}, u32[]{:S(2)}) copy-start(bf16[1,2048,384]{2,1,0:T(8,128)(2,1)} %param.19) | copy-start | bytes 4718596
  7.2 234.9 %reduce-scatter.2.cloned.1.call-start = ((), (), s32[]{:S(2)}) async-start(), calls=%async_computation.6 | async-start | bytes 4456448 | tf_op jit(solution)/shard_map/reduce_scatter | solution.py:140
  18.8 6.1 %copy-start.13 = (f32[256,2]{0,1:T(2,128)S(1)}, f32[256,2]{0,1:T(2,128)}, u32[]{:S(2)}) copy-start(f32[256,2]{0,1:T(2,128)} %param.18) | copy-start | bytes 6148
  29.0 10.8 %copy-start.2 = (bf16[256,2048]{1,0:T(8,128)(2,1)S(1)}, bf16[256,2048]{1,0:T(8,128)(2,1)}, u32[]{:S(2)}) copy-start(bf16[256,2048]{1,0:T(8,128)(2,1)} %param.15) | copy-start | bytes 3145732
  160.5 4.9 %copy-start.4 = (bf16[16,64,4096]{2,1,0:T(8,128)(2,1)}, bf16[16,64,4096]{2,1,0:T(8,128)(2,1)S(1)}, u32[]{:S(2)}) copy-start(bf16[16,64,4096]{2,1,0:T(8,128)(2,1)S(1)} %all_to_all.37) | copy-start | bytes 25165828
  160.5 2.6 copy-start.5
  163.1 2.4 copy-start.16
  163.1 2.6 copy-start.15
  165.7 2.8 copy-start.18
  261.0 4.7 %copy-start.7 = (bf16[128,256]{1,0:T(8,128)(2,1)S(1)}, bf16[128,256]{1,0:T(8,128)(2,1)}, u32[]{:S(2)}) copy-start(bf16[128,256]{1,0:T(8,128)(2,1)} %param.27) | copy-start | bytes 196612
  261.0 4.8 %copy-start.8 = (bf16[128,256]{1,0:T(8,128)(2,1)S(1)}, bf16[128,256]{1,0:T(8,128)(2,1)}, u32[]{:S(2)}) copy-start(bf16[128,256]{1,0:T(8,128)(2,1)} %param.25) | copy-start | bytes 196612
  261.0 5.0 %copy-start.9 = (bf16[128,256]{1,0:T(8,128)(2,1)S(1)}, bf16[128,256]{1,0:T(8,128)(2,1)}, u32[]{:S(2)}) copy-start(bf16[128,256]{1,0:T(8,128)(2,1)} %param.26) | copy-start | bytes 196612
  261.0 5.1 %copy-start.10 = (f32[31,128]{1,0:T(8,128)S(1)}, f32[31,128]{1,0:T(8,128)}, u32[]{:S(2)}) copy-start(f32[31,128]{1,0:T(8,128)} %param.24) | copy-start | bytes 47620
  261.0 98.9 %all-to-all-start.2 = ((bf16[16,16,1,4,2048]{4,3,1,2,0:T(4,128)(2,1)}), bf16[16,16,1,4,2048]{4,3,1,2,0:T(4,128)(2,1)}, u32[]{:S(2)}, u32[]{:S(2)}) async-start(bf16[16,16,1,4,2048]{4,3,1,2,0:T(4,128)(2,1)} %stack.14), calls=%async_computation.3 | async-start | bytes 8388608 | tf_op jit(solution)/shard_map/all_to_all | solution.py:13
  266.1 5.9 %copy-start.17 = (f32[1024,384]{1,0:T(8,128)S(1)}, f32[1024,384]{1,0:T(8,128)}, u32[]{:S(2)}) copy-start(f32[1024,384]{1,0:T(8,128)} %copy-done.16) | copy-start | bytes 4718596
  266.1 5.9 %copy-start.19 = (f32[1024,384]{1,0:T(8,128)S(1)}, f32[1024,384]{1,0:T(8,128)}, u32[]{:S(2)}) copy-start(f32[1024,384]{1,0:T(8,128)} %copy-done.18) | copy-start | bytes 4718596
  402.2 8.7 %copy-start.3 = (bf16[256,2048]{1,0:T(8,128)(2,1)S(1)}, bf16[256,2048]{1,0:T(8,128)(2,1)}, u32[]{:S(2)}) copy-start(bf16[256,2048]{1,0:T(8,128)(2,1)} %param.16) | copy-start | bytes 3145732
  402.2 8.7 %copy-start.6 = (bf16[2048,128]{1,0:T(8,128)(2,1)S(1)}, bf16[2048,128]{1,0:T(8,128)(2,1)}, u32[]{:S(2)}) copy-start(bf16[2048,128]{1,0:T(8,128)(2,1)} %param.22) | copy-start | bytes 1572868
  402.2 8.7 %copy-start.11 = (f32[256]{0:T(256)S(1)}, f32[256]{0:T(256)}, u32[]{:S(2)}) copy-start(f32[256]{0:T(256)} %param.29) | copy-start | bytes 3076
  402.2 8.7 %copy-start.12 = (f32[256]{0:T(256)S(1)}, f32[256]{0:T(256)}, u32[]{:S(2)}) copy-start(f32[256]{0:T(256)} %param.28) | copy-start | bytes 3076
  402.2 8.7 %copy-start.14 = (f32[128]{0:T(128)S(1)}, f32[128]{0:T(128)}, u32[]{:S(2)}) copy-start(f32[128]{0:T(128)} %param.23) | copy-start | bytes 1540
  413.7 12.3 %all-to-all-start.4 = ((f32[16,1,512]{2,1,0:T(1,128)}), f32[16,1,512]{2,1,0:T(1,128)S(1)}, u32[]{:S(2)}, u32[]{:S(2)}) async-start(f32[16,1,512]{2,1,0:T(1,128)} %broadcast_in_dim.51), calls=%async_computation.5 | async-start | bytes 65536 | tf_op jit(solution)/shard_map/all_to_all | solution.py:45
  426.0 18.8 %all-to-all-start.3 = ((bf16[16,128,128]{2,1,0:T(8,128)(2,1)}), bf16[16,128,128]{2,1,0:T(8,128)(2,1)S(1)}, u32[]{:S(2)}, u32[]{:S(2)}) async-start(bf16[16,128,128]{2,1,0:T(8,128)(2,1)} %bitcast.17), calls=%async_computation.4 | async-start | bytes 1048576 | tf_op jit(solution)/shard_map/all_to_all | solution.py:39
  432.1 10.7 %collective-permute-start = (f32[128,30]{0,1:T(8,128)S(1)}, f32[128,30]{0,1:T(8,128)S(1)}, u32[]{:S(2)}, u32[]{:S(2)}) collective-permute-start(f32[128,30]{0,1:T(8,128)S(1)} %slice.271), channel_id=1, source_target_pairs={{16,0},{32,16},{48,32},{64,48},{80,64},{96,80},{112,96},{128,112},... | collective-permute-start | bytes 46088 | tf_op jit(solution)/shard_map/ppermute | solution.py:65
  437.0 8.5 %copy-start.1 = (bf16[1,2048,384]{2,1,0:T(8,128)(2,1)S(1)}, bf16[1,2048,384]{2,1,0:T(8,128)(2,1)}, u32[]{:S(2)}) copy-start(bf16[1,2048,384]{2,1,0:T(8,128)(2,1)} %param.19) | copy-start | bytes 4718596
Sparse Core Ops, SparseCore 0:
  177.7 64.3 reduce-scatter.1
